TPU v7x, 256 devices: a 4x2x16 block of a 4x16x16 slice. The times are simulated.
256 devices in a mesh: grp: 2 (over y), ep: 64 (over z, x), tp: 2 (over core).
Axes of the slice: x: 4, y: 2, z: 16, core: 2. Of those that a mesh axis runs over, the one named last changes fastest.
The devices are a block of a 4x16x16 slice.
Arguments:
- tokens: bfloat16 [32768, 2048], P(('grp', 'ep'), 'tp'), parts along dimension 0, may hold values from -6 to 6
- norm_gain: bfloat16 [2048], P('tp'), may hold values from 0.099609375 to 1.8984375
- w_gate: bfloat16 [64, 2048, 1024], P('ep', None, 'tp'), may hold values from -0.125 to 0.125
- w_up: bfloat16 [64, 2048, 1024], P('ep', None, 'tp'), may hold values from -0.125 to 0.125
- w_down: bfloat16 [64, 1024, 2048], P('ep', 'tp'), may hold values from -0.1875 to 0.1875
- expert_ids: int32 [32768, 2], P(('grp', 'ep')), parts along dimension 0, may hold values from 0 to 63, as said below
- combine: float32 [32768, 2], P(('grp', 'ep')), parts along dimension 0, may hold values from 0.1 to 1
- final_gain: bfloat16 [2048], P('tp'), may hold values from 0.099609375 to 1.8984375
Outputs:
- result: bfloat16 [32768, 2048], P(('grp', 'ep'), 'tp'), parts along dimension 0
There are 2 independent parts, one for each index of `grp`. A program takes and returns all parts, laid end to end along the dimension named above; an argument that names none is the same for every part. Nothing has to cross between parts.
Inputs may be any that keep to these rules, and one draw needn't show every extreme that they name: `expert_ids`: the experts form 4 groups of consecutive ids of equal size; the 2 experts of a row are different and lie in one group. Among the rows of one index of ep no expert is named more than 20 times, and in each such block some expert is named exactly 20 times.
All inputs are finite; a program needn't handle non-finite values.
Results may differ from a plain program's by a relative error of at most 0.0077.
Values may be sent and summed in bfloat16 or wider, within the bound.
No kernel may reach another device: no remote copies, remote signals or barrier semaphores. Data moves between devices by JAX's collectives and lax.ppermute only.
A program may use at most 64 MiB of HBM per device.

v0:
```python
import jax
import jax.numpy as jnp
from jax import lax
from jax.sharding import PartitionSpec as P

GROUPS = 4


def total_of_pieces(x, axis):
    parts = lax.all_gather(x, axis)
    return parts.sum(axis=0)


def split_up(x, dim, count):
    lengths = x.shape
    parts = x.reshape(*lengths[:dim], count, lengths[dim] // count, *lengths[dim + 1 :])
    return jnp.moveaxis(parts, dim, 0)


def sent_and_summed(x, axis, dim):
    parts = split_up(x, dim, lax.axis_size(axis))
    arrived = lax.all_to_all(parts, axis, split_axis=0, concat_axis=0, tiled=True)
    return arrived.astype(jnp.float32).sum(axis=0)


def body(tokens, norm_gain, w_gate, w_up, w_down, expert_ids, combine, final_gain):
    eps = 1e-06
    tok_dev, half = tokens.shape
    n_ep = lax.axis_size("ep")
    n_tp = lax.axis_size("tp")
    width = half * n_tp
    exp_dev = w_gate.shape[0]
    experts = exp_dev * n_ep
    per_group = experts // GROUPS
    capacity = tok_dev // 8 * 5 * 2 // per_group
    top = expert_ids.shape[1]
    narrow = tokens.astype(jnp.float32)
    squares = total_of_pieces(jnp.sum(narrow * narrow, axis=1), "tp")
    scale = lax.rsqrt(squares[:, None] / width + eps)
    normed = (narrow * scale * norm_gain.astype(jnp.float32)).astype(jnp.bfloat16)
    columns = normed.shape[1]
    flat = expert_ids.reshape(-1)
    onehot = (flat[:, None] == jnp.arange(experts, dtype=jnp.int32)[None, :]).astype(jnp.int32)
    ranking = jnp.sum(jnp.cumsum(onehot, axis=0) * onehot, axis=1) - 1
    target = flat * capacity + ranking
    sources = jnp.arange(tok_dev * top, dtype=jnp.int32) // top
    owner = jnp.full((experts * capacity,), tok_dev, jnp.int32).at[target].set(sources)
    padded = jnp.concatenate([normed, jnp.zeros((1, columns), jnp.bfloat16)], axis=0)
    outgoing = padded[owner].reshape(n_ep, exp_dev * capacity, columns)
    arrived = lax.all_to_all(outgoing, "ep", split_axis=0, concat_axis=0, tiled=True)
    rows = (
        arrived.reshape(n_ep, exp_dev, capacity, columns)
        .transpose(1, 0, 2, 3)
        .reshape(exp_dev, n_ep * capacity, columns)
    )
    piece = lax.all_gather(rows, "tp", axis=2, tiled=True)
    gate = jnp.einsum("erd,edf->erf", piece, w_gate, preferred_element_type=jnp.float32)
    upper = jnp.einsum("erd,edf->erf", piece, w_up, preferred_element_type=jnp.float32)
    hidden = (jax.nn.silu(gate) * upper).astype(jnp.bfloat16)
    partial_out = jnp.einsum(
        "erf,efd->erd", hidden, w_down, preferred_element_type=jnp.float32
    ).astype(jnp.bfloat16)
    shares = sent_and_summed(partial_out, "tp", 2).astype(jnp.bfloat16)
    homeward = (
        shares.reshape(exp_dev, n_ep, capacity, half)
        .transpose(1, 0, 2, 3)
        .reshape(n_ep, exp_dev * capacity, half)
    )
    returned = lax.all_to_all(homeward, "ep", split_axis=0, concat_axis=0, tiled=True).reshape(
        experts * capacity, half
    )
    picked = returned[target].astype(jnp.float32).reshape(tok_dev, top, half)
    mixed = jnp.sum(picked * combine[:, :, None], axis=1)
    totals = total_of_pieces(jnp.sum(mixed * mixed, axis=1), "tp")
    norm = lax.rsqrt(totals[:, None] / width + eps)
    return (mixed * norm * final_gain.astype(jnp.float32)).astype(jnp.bfloat16)


def solution(mesh):
    placed = (
        P(("grp", "ep"), "tp"),
        P("tp"),
        P("ep", None, "tp"),
        P("ep", None, "tp"),
        P("ep", "tp", None),
        P(("grp", "ep"), None),
        P(("grp", "ep"), None),
        P("tp"),
    )
    return jax.shard_map(
        body, mesh=mesh, in_specs=placed, out_specs=P(("grp", "ep"), "tp"), check_vma=False
    )
```

profile of v0, /device:TPU:33, one launch (start us, length us, event | category | flops | bytes accessed | tf_op | source)
XLA Modules:
  0.0 464.1 jit_solution(18118570353789319803)
XLA Ops:
  6.5 0.0 copy-start
  6.6 0.0 all-gather.6.cloned.1.call-start
  6.6 1.0 copy.16
  7.5 0.1 eq.29
  7.7 0.1 eq.25
  7.8 0.7 broadcast_multiply_fusion
  8.5 1.2 reduce-window.6
  9.7 0.2 slice_reduce_fusion
  10.0 0.1 fusion.21
  10.1 0.1 copy.15
  10.3 0.1 mul.81
  10.4 2.5 scatter_custom_fusion
  12.9 1.2 fusion.17
  14.1 21.9 %all-gather.2 = f32[2,1,256]{2,1,0:T(1,128)S(1)} all-gather(f32[1,1,256]{2,1,0:T(1,128)S(1)} %bitcast.48), channel_id=2, replica_groups=mesh['grp'=2,'ep'=64,'tp'=2] {'tp'}, dimensions={0}, use_global_device_ids=true | all-gather | bytes 3072 | tf_op jit(solution)/shard_map/all_gather | solution.py:10
  36.1 0.7 convert_element_type.38
  36.8 1.2 fusion.19
  38.1 5.1 %gather_fusion = bf16[1280,1024]{1,0:T(8,128)(2,1)} fusion(bf16[257,1024]{1,0:T(8,128)(2,1)S(1)} %concatenate.3, s32[2048]{0:T(1024)S(1)} %pad_clamp_fusion), kind=kCustom, calls=%fused_computation | custom fusion | bytes 5248000 | tf_op jit(solution)/shard_map/gather | solution.py:49
  43.1 5.2 %reshape.113 = bf16[64,20,1024]{2,1,0:T(8,128)(2,1)} reshape(bf16[1280,1024]{1,0:T(8,128)(2,1)} %gather_fusion) | data formatting | bytes 5242880 | tf_op jit(solution)/shard_map/reshape | solution.py:49
  48.3 149.8 %all_to_all.15 = bf16[64,20,1024]{2,1,0:T(8,128)(2,1)} all-to-all(bf16[64,20,1024]{2,1,0:T(8,128)(2,1)} %reshape.113), channel_id=1, replica_groups=mesh['grp'=2,'ep'=64,'tp'=2] {'ep'}, dimensions={0} | all-to-all | bytes 5242880 | tf_op jit(solution)/shard_map/all_to_all | solution.py:50
  198.1 5.2 %reshape_transpose_reshape.6 = bf16[1,1280,1024]{2,1,0:T(8,128)(2,1)} reshape(bf16[64,20,1024]{2,1,0:T(8,128)(2,1)} %all_to_all.15) | data formatting | bytes 5242880 | tf_op jit(solution)/shard_map/reshape;transpose;reshape | solution.py:54
  203.3 0.1 all-gather.6.cloned.1.call-update
  203.3 21.7 %all-gather.6.cloned.1.call-done = bf16[1,1280,2048]{2,1,0:T(8,128)(2,1)} async-done(((bf16[1,1280,1024]{2,1,0:T(8,128)(2,1)}), bf16[1,1280,2048]{2,1,0:T(8,128)(2,1)}) %all-gather.6.cloned.1.call-update) | async-done | bytes 5242896 | tf_op jit(solution)/shard_map/all_gather | solution.py:56
  225.0 7.6 %fusion.2 = f32[1280,512]{1,0:T(8,128)} fusion(bf16[1,1280,2048]{2,1,0:T(8,128)(2,1)} %all-gather.6.cloned.1.call-done, bf16[1,2048,512]{2,1,0:T(8,128)(2,1)} %param.10), kind=kOutput, calls=%fused_computation.6 | convolution fusion | flops 2684354560 | bytes 9961472 | tf_op jit(solution)/shard_map/erd,edf->erf/dot_general | solution.py:57
  232.6 0.0 copy-done
  232.6 10.3 %convolution_convert_fusion = bf16[1280,2048]{1,0:T(8,128)(2,1)} fusion(bf16[1,512,2048]{2,1,0:T(8,128)(2,1)S(1)} %copy-done, bf16[1,1280,2048]{2,1,0:T(8,128)(2,1)} %all-gather.6.cloned.1.call-done, f32[1280,512]{1,0:T(8,128)} %fusion.2, bf16[1,2048,512]{2,1,0:T(8,128)(2,1)} %param.11), kind=kOutput, calls=%fused_computation.3 | convolution fusion | flops 5375262720 | bytes 17301504 | tf_op jit(solution)/shard_map/erf,efd->erd/dot_general | solution.py:60
  242.9 9.5 %reshape.118 = bf16[1,1280,2,1024]{3,2,1,0:T(2,128)(2,1)} reshape(bf16[1280,2048]{1,0:T(8,128)(2,1)} %convolution_convert_fusion) | data formatting | bytes 10485760 | tf_op jit(solution)/shard_map/reshape | solution.py:16
  252.4 4.1 copy.24
  256.5 9.0 %all_to_all.16 = bf16[2,1,1280,1024]{3,2,1,0:T(8,128)(2,1)} all-to-all(bf16[2,1,1280,1024]{3,2,1,0:T(8,128)(2,1)S(1)} %bitcast.44), channel_id=1, replica_groups=mesh['grp'=2,'ep'=64,'tp'=2] {'tp'}, dimensions={0} | all-to-all | bytes 10485760 | tf_op jit(solution)/shard_map/all_to_all | solution.py:22
  265.5 6.2 %reduce_sum.69 = bf16[1280,1024]{1,0:T(8,128)(2,1)} reduce(bf16[2,1,1280,1024]{3,2,1,0:T(8,128)(2,1)} %all_to_all.16, bf16[]{:T(256)} %constant.38.clone.1), dimensions={0,1}, to_apply=%region_6.7 | reduce | flops 1310720 | bytes 7864322 | tf_op jit(solution)/shard_map/reduce_sum | solution.py:23
  271.7 5.1 %reshape_transpose_reshape.7 = bf16[64,20,1024]{2,1,0:T(8,128)(2,1)} reshape(bf16[1280,1024]{1,0:T(8,128)(2,1)} %reduce_sum.69) | data formatting | bytes 5242880 | tf_op jit(solution)/shard_map/reshape;transpose;reshape | solution.py:67
  276.9 0.0 copy-start.1
  276.9 0.0 copy-start.2
  276.9 16.3 %all-to-all-start.2 = ((bf16[64,20,1024]{2,1,0:T(8,128)(2,1)}), bf16[64,20,1024]{2,1,0:T(8,128)(2,1)}, u32[]{:S(2)}, u32[]{:S(2)}) async-start(bf16[64,20,1024]{2,1,0:T(8,128)(2,1)} %reshape_transpose_reshape.7), calls=%async_computation.2 | async-start | bytes 6291456 | tf_op jit(solution)/shard_map/all_to_all | solution.py:69
  293.2 0.0 copy-done.1
  293.2 0.1 copy.20
  293.3 0.0 copy-done.2
  293.4 138.9 %all-to-all-done.2 = bf16[64,20,1024]{2,1,0:T(8,128)(2,1)} async-done(((bf16[64,20,1024]{2,1,0:T(8,128)(2,1)}), bf16[64,20,1024]{2,1,0:T(8,128)(2,1)}, u32[]{:S(2)}, u32[]{:S(2)}) %all-to-all-start.2) | async-done | bytes 2621472 | tf_op jit(solution)/shard_map/all_to_all | solution.py:69
  432.3 5.2 %reshape.119 = bf16[1280,1024]{1,0:T(8,128)(2,1)} reshape(bf16[64,20,1024]{2,1,0:T(8,128)(2,1)} %all-to-all-done.2) | data formatting | bytes 5242880 | tf_op jit(solution)/shard_map/reshape | solution.py:69
  437.4 4.8 %gather_fusion.1 = bf16[512,1024]{1,0:T(8,128)(2,1)S(1)} fusion(bf16[1280,1024]{1,0:T(8,128)(2,1)} %reshape.119, s32[1024]{0:T(1024)S(1)} %pad_clamp_fusion.1), kind=kCustom, calls=%fused_computation.1 | custom fusion | bytes 2099200 | tf_op jit(solution)/shard_map/gather | solution.py:72
  442.2 2.4 reshape.120
  444.6 4.3 multiply_reduce_fusion
  448.9 0.1 multiply_reduce_fusion.1
  449.1 7.2 %all-gather.3 = f32[2,1,256]{2,1,0:T(1,128)S(1)} all-gather(f32[1,1,256]{2,1,0:T(1,128)S(1)} %bitcast.49), channel_id=3, replica_groups=mesh['grp'=2,'ep'=64,'tp'=2] {'tp'}, dimensions={0}, use_global_device_ids=true | all-gather | bytes 3072 | tf_op jit(solution)/shard_map/all_gather | solution.py:10
  456.2 1.0 multiply_convert_fusion
  (15 shorter events, 0.2 us)
Async XLA Ops:
  6.5 226.0 %copy-start = (bf16[1,512,2048]{2,1,0:T(8,128)(2,1)S(1)}, bf16[1,512,2048]{2,1,0:T(8,128)(2,1)}, u32[]{:S(2)}) copy-start(bf16[1,512,2048]{2,1,0:T(8,128)(2,1)} %param.12) | copy-start | bytes 6291460
  6.6 218.5 %all-gather.6.cloned.1.call-start = ((), (), s32[]{:S(2)}) async-start(), calls=%async_computation.3 | async-start | bytes 7864320 | tf_op jit(solution)/shard_map/all_gather | solution.py:56
  276.9 16.3 %copy-start.1 = (f32[256,2]{0,1:T(2,128)S(1)}, f32[256,2]{0,1:T(2,128)}, u32[]{:S(2)}) copy-start(f32[256,2]{0,1:T(2,128)} %param.14) | copy-start | bytes 6148
  276.9 16.5 %copy-start.2 = (bf16[1024]{0:T(1024)(128)(2,1)S(1)}, bf16[1024]{0:T(1024)(128)(2,1)}, u32[]{:S(2)}) copy-start(bf16[1024]{0:T(1024)(128)(2,1)} %param.15) | copy-start | bytes 6148
  276.9 155.4 %all-to-all-start.2 = ((bf16[64,20,1024]{2,1,0:T(8,128)(2,1)}), bf16[64,20,1024]{2,1,0:T(8,128)(2,1)}, u32[]{:S(2)}, u32[]{:S(2)}) async-start(bf16[64,20,1024]{2,1,0:T(8,128)(2,1)} %reshape_transpose_reshape.7), calls=%async_computation.2 | async-start | bytes 6291456 | tf_op jit(solution)/shard_map/all_to_all | solution.py:69
Sparse Core Ops, SparseCore 0:
  203.4 21.5 all-gather.5
where the time goes:
time: 465 us; the launch traced here: 464 us
  blocking collectives  188 us (40%)
  waiting for transfers between devices  161 us (35%)
  local copies, waits for them, and re-layouts  50.9 us (11%)
  matrix products  17.9 us (4%)
  other arithmetic  16.9 us (4%)
  starting transfers between devices  16.3 us (4%)
  between operations  13.6 us (3%)
    all_to_all x1, blocking collectives, body(): lax.all_to_all(outgoing, 'ep', split_axis=0, concat_axis=0, tiled=True)  150 us
    all_to_all x1, waiting for transfers between devices, body(): lax.all_to_all(homeward, 'ep', split_axis=0, concat_axis=0, tiled=True)  139 us
    all_gather x2, blocking collectives, total_of_pieces(): parts = lax.all_gather(x, axis)  29.1 us
    all_gather x1, waiting for transfers between devices, body(): piece = lax.all_gather(rows, 'tp', axis=2, tiled=True)  21.7 us
    all_to_all x1, starting transfers between devices, body(): lax.all_to_all(homeward, 'ep', split_axis=0, concat_axis=0, tiled=True)  16.3 us
    reshape x2, local copies, waits for them, and re-layouts, split_up(): x.reshape(*lengths[:dim], count, lengths[dim] // count, *lengths[dim + 1:])  13.6 us
    dot_general x1, matrix products, body(): jnp.einsum('erf,efd->erd', hidden, w_down, preferred_element_type=jnp.flo...  10.3 us
  transfers between devices with their start and end apart: 2, of which 2 were waited for; matrix products, arithmetic and copies ran while one was open for 0% of the time, Pallas kernels for 0%

commit v1 on v0

--- a/solution.py
+++ b/solution.py
@@ -53,7 +53,9 @@
         .transpose(1, 0, 2, 3)
         .reshape(exp_dev, n_ep * capacity, columns)
     )
-    piece = lax.all_gather(rows, "tp", axis=2, tiled=True)
+    piece = jnp.concatenate(
+        lax.all_to_all(jnp.stack([rows] * lax.axis_size("tp")), "tp", 0, 0), axis=2
+    )
     gate = jnp.einsum("erd,edf->erf", piece, w_gate, preferred_element_type=jnp.float32)
     upper = jnp.einsum("erd,edf->erf", piece, w_up, preferred_element_type=jnp.float32)
     hidden = (jax.nn.silu(gate) * upper).astype(jnp.bfloat16)

time: 465 us -> 440 us (0.946)
  waiting for transfers between devices: 161 us -> 139 us
  between operations: 13.6 us -> 0.18 us
  blocking collectives: 188 us -> 201 us
  starting transfers between devices: 16.3 us -> 7.6 us
    all_gather x1 -> x0, waiting for transfers between devices: 21.7 us -> none  [body(): piece = lax.all_gather(rows, 'tp', axis=2, tiled=True)]
    all_to_all x0 -> x1, blocking collectives: none -> 13.6 us  [body(): lax.all_to_all(jnp.stack([rows] * lax.axis_size('tp')), 'tp', 0, 0)]
    all_to_all x1, starting transfers between devices: 16.3 us -> 7.6 us  [body(): lax.all_to_all(homeward, 'ep', split_axis=0, concat_axis=0, tiled=True)]
    reshape x0 -> x1, local copies, waits for them, and re-layouts: none -> 7.92 us  [body(): jnp.concatenate(lax.all_to_all(jnp.stack([rows] * lax.axis_size('tp')), '...]
  transfers between devices with their start and end apart: 2 -> 1, of which waited for: 2 -> 1; matrix products, arithmetic and copies ran while one was open for 0% -> 0% of each run, Pallas kernels for 0% -> 0%
where the time goes in v1:
time: 440 us; the launch traced here: 438 us
  blocking collectives  201 us (46%)
  waiting for transfers between devices  139 us (32%)
  local copies, waits for them, and re-layouts  53.7 us (12%)
  other arithmetic  18.8 us (4%)
  matrix products  17.9 us (4%)
  starting transfers between devices  7.6 us (2%)
    all_to_all x1, blocking collectives, body(): lax.all_to_all(outgoing, 'ep', split_axis=0, concat_axis=0, tiled=True)  150 us
    all_to_all x1, waiting for transfers between devices, body(): lax.all_to_all(homeward, 'ep', split_axis=0, concat_axis=0, tiled=True)  139 us
    all_gather x2, blocking collectives, total_of_pieces(): parts = lax.all_gather(x, axis)  28.4 us
    reshape x2, local copies, waits for them, and re-layouts, split_up(): x.reshape(*lengths[:dim], count, lengths[dim] // count, *lengths[dim + 1:])  13.6 us
    all_to_all x1, blocking collectives, body(): lax.all_to_all(jnp.stack([rows] * lax.axis_size('tp')), 'tp', 0, 0)  13.6 us
    dot_general x1, matrix products, body(): jnp.einsum('erf,efd->erd', hidden, w_down, preferred_element_type=jnp.flo...  10.3 us
    all_to_all x1, blocking collectives, sent_and_summed(): lax.all_to_all(parts, axis, split_axis=0, concat_axis=0, tiled=True)  9.02 us
  transfers between devices with their start and end apart: 1, of which 1 were waited for; matrix products, arithmetic and copies ran while one was open for 0% of the time, Pallas kernels for 0%

profile of v1, /device:TPU:33, one launch (start us, length us, event | category | flops | bytes accessed | tf_op | source)
XLA Modules:
  0.0 438.3 jit_solution(13814672209699792496)
XLA Ops:
  0.0 0.0 copy-start
  0.0 1.0 copy.17
  1.0 0.1 eq.29
  1.1 0.1 eq.25
  1.3 0.7 broadcast_multiply_fusion
  2.0 1.2 reduce-window.6
  3.2 0.2 slice_reduce_fusion
  3.4 0.1 fusion.11
  3.6 0.1 copy.16
  3.7 0.1 mul.81
  3.9 2.5 scatter_custom_fusion
  6.4 1.2 fusion.5
  7.6 21.9 %all-gather.2 = f32[2,1,256]{2,1,0:T(1,128)S(1)} all-gather(f32[1,1,256]{2,1,0:T(1,128)S(1)} %bitcast.44), channel_id=2, replica_groups=mesh['grp'=2,'ep'=64,'tp'=2] {'tp'}, dimensions={0}, use_global_device_ids=true | all-gather | bytes 3072 | tf_op jit(solution)/shard_map/all_gather | solution.py:10
  29.5 0.7 convert_element_type.38
  30.2 1.2 fusion.7
  31.5 5.1 %gather_fusion = bf16[1280,1024]{1,0:T(8,128)(2,1)} fusion(bf16[257,1024]{1,0:T(8,128)(2,1)S(1)} %concatenate.3, s32[2048]{0:T(1024)S(1)} %pad_clamp_fusion), kind=kCustom, calls=%fused_computation | custom fusion | bytes 5248000 | tf_op jit(solution)/shard_map/gather | solution.py:49
  36.6 5.2 %reshape.119 = bf16[64,20,1024]{2,1,0:T(8,128)(2,1)} reshape(bf16[1280,1024]{1,0:T(8,128)(2,1)} %gather_fusion) | data formatting | bytes 5242880 | tf_op jit(solution)/shard_map/reshape | solution.py:49
  41.8 149.8 %all_to_all.20 = bf16[64,20,1024]{2,1,0:T(8,128)(2,1)} all-to-all(bf16[64,20,1024]{2,1,0:T(8,128)(2,1)} %reshape.119), channel_id=1, replica_groups=mesh['grp'=2,'ep'=64,'tp'=2] {'ep'}, dimensions={0} | all-to-all | bytes 5242880 | tf_op jit(solution)/shard_map/all_to_all | solution.py:50
  191.5 5.2 %stack_reshape_transpose_reshape.4 = bf16[1,1,1280,1024]{3,2,1,0:T(8,128)(2,1)} reshape(bf16[64,20,1024]{2,1,0:T(8,128)(2,1)} %all_to_all.20) | data formatting | bytes 5242880 | tf_op jit(solution)/shard_map/stack;reshape;transpose;reshape | solution.py:57
  196.7 3.0 pad_maximum_fusion
  199.7 13.6 %all_to_all.21 = bf16[2,1,1280,1024]{3,2,1,0:T(8,128)(2,1)} all-to-all(bf16[2,1,1280,1024]{3,2,1,0:T(8,128)(2,1)S(1)} %pad_maximum_fusion), channel_id=1, replica_groups=mesh['grp'=2,'ep'=64,'tp'=2] {'tp'}, dimensions={0} | all-to-all | bytes 10485760 | tf_op jit(solution)/shard_map/all_to_all | solution.py:57
  213.3 7.9 %copy.20 = bf16[1,1280,2,1024]{1,3,2,0:T(8,128)(2,1)} copy(bf16[1,1280,2,1024]{3,1,0,2:T(8,128)(2,1)} %bitcast.37) | data formatting | bytes 10485760 | tf_op jit(solution)/shard_map/reshape | solution.py:56
  221.2 7.6 %fusion.3 = f32[1280,512]{1,0:T(8,128)} fusion(bf16[1280,2048]{0,1:T(8,128)(2,1)} %bitcast.39, bf16[1,2048,512]{2,1,0:T(8,128)(2,1)} %param.10), kind=kOutput, calls=%fused_computation.10 | convolution fusion | flops 2684354560 | bytes 9961472 | tf_op jit(solution)/shard_map/erd,edf->erf/dot_general | solution.py:59
  228.8 0.0 copy-done
  228.8 10.3 %convolution_convert_fusion = bf16[1280,2048]{1,0:T(8,128)(2,1)} fusion(bf16[1,512,2048]{2,1,0:T(8,128)(2,1)S(1)} %copy-done, bf16[1280,2048]{0,1:T(8,128)(2,1)} %bitcast.40, f32[1280,512]{1,0:T(8,128)} %fusion.3, bf16[1,2048,512]{2,1,0:T(8,128)(2,1)} %param.11), kind=kOutput, calls=%fused_computation.3 | convolution fusion | flops 5375262720 | bytes 17301504 | tf_op jit(solution)/shard_map/erf,efd->erd/dot_general | solution.py:62
  239.1 9.5 %reshape.125 = bf16[1,1280,2,1024]{3,2,1,0:T(2,128)(2,1)} reshape(bf16[1280,2048]{1,0:T(8,128)(2,1)} %convolution_convert_fusion) | data formatting | bytes 10485760 | tf_op jit(solution)/shard_map/reshape | solution.py:16
  248.6 4.1 copy.26
  252.8 9.0 %all_to_all.22 = bf16[2,1,1280,1024]{3,2,1,0:T(8,128)(2,1)} all-to-all(bf16[2,1,1280,1024]{3,2,1,0:T(8,128)(2,1)S(1)} %bitcast.38), channel_id=1, replica_groups=mesh['grp'=2,'ep'=64,'tp'=2] {'tp'}, dimensions={0} | all-to-all | bytes 10485760 | tf_op jit(solution)/shard_map/all_to_all | solution.py:22
  261.8 5.1 %reduce_sum.69 = bf16[1280,1024]{1,0:T(8,128)(2,1)S(1)} reduce(bf16[2,1,1280,1024]{3,2,1,0:T(8,128)(2,1)} %all_to_all.22, bf16[]{:T(256)} %constant.38.clone.1), dimensions={0,1}, to_apply=%region_6.7 | reduce | flops 1310720 | bytes 7864322 | tf_op jit(solution)/shard_map/reduce_sum | solution.py:23
  266.9 2.4 reshape_transpose_reshape.3
  269.3 0.0 copy-start.2
  269.3 0.0 copy-start.3
  269.3 7.6 %all-to-all-start.3 = ((bf16[64,20,1024]{2,1,0:T(8,128)(2,1)}), bf16[64,20,1024]{2,1,0:T(8,128)(2,1)}, u32[]{:S(2)}, u32[]{:S(2)}) async-start(bf16[64,20,1024]{2,1,0:T(8,128)(2,1)} %reshape_transpose_reshape.3), calls=%async_computation.3 | async-start | bytes 6291456 | tf_op jit(solution)/shard_map/all_to_all | solution.py:71
  276.9 0.0 copy-done.2
  276.9 0.1 copy.22
  277.0 0.0 copy-done.3
  277.1 139.3 %all-to-all-done.3 = bf16[64,20,1024]{2,1,0:T(8,128)(2,1)} async-done(((bf16[64,20,1024]{2,1,0:T(8,128)(2,1)}), bf16[64,20,1024]{2,1,0:T(8,128)(2,1)}, u32[]{:S(2)}, u32[]{:S(2)}) %all-to-all-start.3) | async-done | bytes 2621472 | tf_op jit(solution)/shard_map/all_to_all | solution.py:71
  416.4 3.6 reshape.126
  420.0 2.8 gather_fusion.1
  422.8 0.0 copy-start.1
  422.8 3.5 reshape.127
  426.4 4.3 multiply_reduce_fusion
  430.7 0.1 multiply_reduce_fusion.1
  430.8 6.5 %all-gather.3 = f32[2,1,256]{2,1,0:T(1,128)S(1)} all-gather(f32[1,1,256]{2,1,0:T(1,128)S(1)} %bitcast.45), channel_id=3, replica_groups=mesh['grp'=2,'ep'=64,'tp'=2] {'tp'}, dimensions={0}, use_global_device_ids=true | all-gather | bytes 3072 | tf_op jit(solution)/shard_map/all_gather | solution.py:10
  437.4 1.0 multiply_convert_fusion
  438.3 0.0 copy-done.1
  (15 shorter events, 0.2 us)
Async XLA Ops:
  0.0 228.8 %copy-start = (bf16[1,512,2048]{2,1,0:T(8,128)(2,1)S(1)}, bf16[1,512,2048]{2,1,0:T(8,128)(2,1)}, u32[]{:S(2)}) copy-start(bf16[1,512,2048]{2,1,0:T(8,128)(2,1)} %param.12) | copy-start | bytes 6291460
  269.3 7.6 %copy-start.2 = (f32[256,2]{0,1:T(2,128)S(1)}, f32[256,2]{0,1:T(2,128)}, u32[]{:S(2)}) copy-start(f32[256,2]{0,1:T(2,128)} %param.14) | copy-start | bytes 6148
  269.3 7.8 %copy-start.3 = (bf16[1024]{0:T(1024)(128)(2,1)S(1)}, bf16[1024]{0:T(1024)(128)(2,1)}, u32[]{:S(2)}) copy-start(bf16[1024]{0:T(1024)(128)(2,1)} %param.15) | copy-start | bytes 6148
  269.3 147.1 %all-to-all-start.3 = ((bf16[64,20,1024]{2,1,0:T(8,128)(2,1)}), bf16[64,20,1024]{2,1,0:T(8,128)(2,1)}, u32[]{:S(2)}, u32[]{:S(2)}) async-start(bf16[64,20,1024]{2,1,0:T(8,128)(2,1)} %reshape_transpose_reshape.3), calls=%async_computation.3 | async-start | bytes 6291456 | tf_op jit(solution)/shard_map/all_to_all | solution.py:71
  422.8 15.5 %copy-start.1 = (bf16[1,512,2048]{2,1,0:T(8,128)(2,1)S(1)}, bf16[1,512,2048]{2,1,0:T(8,128)(2,1)}, u32[]{:S(2)}) copy-start(bf16[1,512,2048]{2,1,0:T(8,128)(2,1)} %param.12) | copy-start | bytes 6291460
